TPU v7x, 32 devices: a whole 2x2x4 slice. The times are simulated.
32 devices in a mesh: grp: 2 (over y), sp: 4 (over z), tp: 4 (over x, core).
Axes of the slice: x: 2, y: 2, z: 4, core: 2. Of those that a mesh axis runs over, the one named last changes fastest.
Arguments:
- tokens: bfloat16 [3072, 2048], P(('grp', 'sp')), parts along dimension 0, may hold values from -6 to 6
- norm_gain: float32 [2, 2048], replicated, may hold values from 0.1 to 1.9
- entry_weight: bfloat16 [2, 2048, 2048], P(None, 'sp', 'tp'), may hold values from -0.125 to 0.125
- mix_weight: bfloat16 [2, 4, 512, 512], P(None, 'tp'), may hold values from -0.25 to 0.25
- pool_gain: float32 [2, 2048], P(None, 'tp'), may hold values from 0.1 to 1.9
- back_weight: bfloat16 [2, 2048, 2048], P(None, 'tp', 'sp'), may hold values from -0.25 to 0.25
Outputs:
- result_tokens: bfloat16 [3072, 2048], P(('grp', 'sp')), parts along dimension 0
There are 2 independent parts, one for each index of `grp`. A program takes and returns all parts, laid end to end along the dimension named above; an argument that names none is the same for every part. Nothing has to cross between parts.
All inputs are finite; a program needn't handle non-finite values.
Results may differ from a plain program's by a relative error of at most 0.018.
Values may be sent and summed in bfloat16 or wider, within the bound.
A program may use at most 64 MiB of HBM per device.

v0:
```python
import jax
import jax.numpy as jnp
from jax import lax
from jax.sharding import PartitionSpec as P

GROUPS = 4
LAYERS = 2


EPSILON = 1e-05


def extended_2(value, sides, width):
    for axis, dim in sides:
        size, length = (lax.axis_size(axis), value.shape[dim])
        up = [(i, (i + 1) % size) for i in range(size - 1)]
        down = [(j, i) for i, j in up]
        last = lax.slice_in_dim(value, length - width, length, axis=dim)
        first = lax.slice_in_dim(value, 0, width, axis=dim)
        before = lax.ppermute(last, axis, up)
        after = lax.ppermute(first, axis, down)
        value = jnp.concatenate([before, value, after], axis=dim)
    return value


def window_mean(padded, positions, halves, total_length, reach):
    row_count = positions.shape[0]
    summed = jnp.zeros((row_count,) + padded.shape[1:], jnp.float32)
    for offset in range(-reach, reach):
        inside = ((offset >= -halves) & (offset < halves)).astype(jnp.float32)
        summed = (
            summed + padded[reach + offset : reach + offset + row_count] * inside[None, :, None]
        )
    lower = jnp.maximum(positions[:, None] - halves[None, :], 0)
    upper = jnp.minimum(positions[:, None] + halves[None, :], total_length)
    counted = (upper - lower).astype(jnp.float32)
    return summed / counted[:, :, None]


def normalize(state, gain):
    values = state.astype(jnp.float32)
    scaled = values * lax.rsqrt(jnp.mean(values * values, axis=-1, keepdims=True) + EPSILON)
    return (scaled * gain).astype(jnp.bfloat16)


def pool_groups(pooled_in, mix_layer, gain_layer, reach):
    row_count = pooled_in.shape[0]
    group_here = mix_layer.shape[0]
    width = mix_layer.shape[1]
    extended = extended_2(pooled_in, (("sp", 0),), reach)
    first_group = lax.axis_index("tp") * group_here
    halves = jnp.left_shift(jnp.int32(1), first_group + jnp.arange(group_here, dtype=jnp.int32))
    positions = lax.axis_index("sp") * row_count + jnp.arange(row_count, dtype=jnp.int32)
    total_length = lax.axis_size("sp") * row_count
    padded = extended.reshape(row_count + 2 * reach, group_here, width).astype(jnp.float32)
    means = window_mean(padded, positions, halves, total_length, reach)
    differ = (means - padded[reach : reach + row_count]).astype(jnp.bfloat16)
    mixed = jnp.einsum("tgc,gcd->tgd", differ, mix_layer, preferred_element_type=jnp.float32)
    return (mixed.reshape(row_count, group_here * width) * gain_layer).astype(jnp.bfloat16)


def per_device(tokens, norm_gain, entry_weight, mix_weight, pool_gain, back_weight):
    reach = 2 ** (GROUPS - 1)
    state = tokens
    entry_all, back_all = (
        lax.all_gather(entry_weight, "sp", axis=1, tiled=True),
        lax.all_gather(back_weight, "sp", axis=2, tiled=True),
    )
    for layer in range(LAYERS):
        normed = normalize(state, norm_gain[layer])
        pooled_in = jnp.dot(normed, entry_all[layer], preferred_element_type=jnp.float32).astype(
            jnp.bfloat16
        )
        back_local = back_all[layer]
        mixed = pool_groups(pooled_in, mix_weight[layer], pool_gain[layer], reach)
        update = jnp.dot(mixed, back_local, preferred_element_type=jnp.float32)
        summed = lax.psum(update.astype(jnp.bfloat16), "tp").astype(jnp.float32)
        state = (state.astype(jnp.float32) + summed).astype(jnp.bfloat16)
    return state


def solution(mesh):
    return jax.shard_map(
        per_device,
        mesh=mesh,
        in_specs=(
            P(("grp", "sp"), None),
            P(),
            P(None, "sp", "tp"),
            P(None, "tp", None, None),
            P(None, "tp"),
            P(None, "tp", "sp"),
        ),
        out_specs=P(("grp", "sp"), None),
        check_vma=False,
    )
```

profile of v0, /device:TPU:11, one launch (start us, length us, event | category | flops | bytes accessed | tf_op | source)
XLA Modules:
  0.0 295.5 jit_solution(13952838582287595426)
XLA Ops:
  6.5 0.7 all-gather.3.cloned.1.call-update
  7.3 0.0 all-gather.5.cloned.1.call-start
  7.3 0.7 all-gather.5.cloned.1.call-update
  8.0 0.0 all-reduce.3.cloned.1.call-start
  8.1 0.4 fusion
  8.5 79.7 %all-gather.3.cloned.1.call-done = bf16[2,2048,512]{2,1,0:T(8,128)(2,1)} async-done(((bf16[2,512,512]{2,1,0:T(8,128)(2,1)}), bf16[2,2048,512]{2,1,0:T(8,128)(2,1)}) %all-gather.3.cloned.1.call-update) | async-done | bytes 4194320 | tf_op jit(solution)/shard_map/all_gather | solution.py:66
  88.2 2.6 fusion.20
  90.8 4.1 %collective-permute-start = (bf16[8,512]{1,0:T(8,128)(2,1)S(1)}, bf16[8,512]{1,0:T(8,128)(2,1)S(1)}, u32[]{:S(2)}, u32[]{:S(2)}) collective-permute-start(bf16[8,512]{1,0:T(8,128)(2,1)S(1)} %get-tuple-element.7), channel_id=1, source_target_pairs={{0,4},{4,8},{8,12},{1,5},{5,9},{9,13},{2,6},{6,10},{10,14},{3,7},{... | collective-permute-start | bytes 24584 | tf_op jit(solution)/shard_map/ppermute | solution.py:20
  94.9 1.9 collective-permute-start.1
  97.0 2.3 collective-permute-done.1
  99.3 0.1 maximum_convert_fusion
  99.4 69.6 %all-gather.5.cloned.1.call-done = bf16[2,512,2048]{2,1,0:T(8,128)(2,1)} async-done(((bf16[2,512,512]{2,1,0:T(8,128)(2,1)}), bf16[2,512,2048]{2,1,0:T(8,128)(2,1)}) %all-gather.5.cloned.1.call-update) | async-done | bytes 4194320 | tf_op jit(solution)/shard_map/all_gather | solution.py:67
  169.0 5.3 %convolution_convert_fusion.1 = bf16[384,2048]{1,0:T(8,128)(2,1)} fusion(bf16[2,512,2048]{2,1,0:T(8,128)(2,1)} %all-gather.5.cloned.1.call-done, bf16[2,1,512,512]{3,2,1,0:T(8,128)(2,1)} %param.9, f32[512]{0:T(512)S(1)} %bitcast.87, f32[400,1,512]{2,0,1:T(8,128)S(1)} %maximum_convert_fusion, f32[384]{0:T(512)S(1)} %subtract_convert_fusion, f32[]{:T(128)S(6)} %mul.373, ...), kind=kOutput, calls=%fused_computation.15 | convolution fusion | flops 1014497280 | bytes 16781376 | tf_op jit(solution)/shard_map/dot_general | solution.py:76
  174.3 0.0 all-reduce.5.cloned.1.call-start
  174.4 43.1 %all-reduce.3.cloned.1.call-done = bf16[384,2048]{1,0:T(8,128)(2,1)} async-done(((bf16[384,2048]{1,0:T(8,128)(2,1)}), bf16[384,2048]{1,0:T(8,128)(2,1)}) %all-reduce.3.cloned.1.call-update) | async-done | bytes 1572880 | tf_op jit(solution)/shard_map/psum | solution.py:77
  217.5 2.1 fusion.4
  219.6 2.6 fusion.23
  222.2 3.1 %collective-permute-start.2 = (bf16[8,512]{1,0:T(8,128)(2,1)S(1)}, bf16[8,512]{1,0:T(8,128)(2,1)S(1)}, u32[]{:S(2)}, u32[]{:S(2)}) collective-permute-start(bf16[8,512]{1,0:T(8,128)(2,1)S(1)} %get-tuple-element.5), channel_id=1, source_target_pairs={{0,4},{4,8},{8,12},{1,5},{5,9},{9,13},{2,6},{6,10},{10,14},{3,7},{... | collective-permute-start | bytes 24584 | tf_op jit(solution)/shard_map/ppermute | solution.py:20
  225.3 2.2 collective-permute-start.3
  227.5 2.2 collective-permute-done.3
  229.7 1.0 maximum_convert_fusion.1
  230.8 11.3 %convolution_convert_fusion = bf16[384,2048]{1,0:T(8,128)(2,1)} fusion(bf16[2,512,2048]{2,1,0:T(8,128)(2,1)} %all-gather.5.cloned.1.call-done, bf16[2,1,512,512]{3,2,1,0:T(8,128)(2,1)} %param.9, f32[512]{0:T(512)S(1)} %bitcast.86, f32[400,1,512]{2,0,1:T(8,128)} %maximum_convert_fusion.1, f32[384]{0:T(512)S(1)} %subtract_convert_fusion, f32[]{:T(128)S(6)} %mul.373, ...), kind=kOutput, calls=%fused_computation.14 | convolution fusion | flops 1014497280 | bytes 16780864 | tf_op jit(solution)/shard_map/dot_general | solution.py:76
  242.0 43.6 %all-reduce.5.cloned.1.call-done = bf16[384,2048]{1,0:T(8,128)(2,1)} async-done(((bf16[384,2048]{1,0:T(8,128)(2,1)}), bf16[384,2048]{1,0:T(8,128)(2,1)}) %all-reduce.5.cloned.1.call-update) | async-done | bytes 1572880 | tf_op jit(solution)/shard_map/psum | solution.py:77
  285.6 3.4 %fusion.7 = bf16[384,2048]{1,0:T(8,128)(2,1)} fusion(bf16[384,2048]{1,0:T(8,128)(2,1)} %all-reduce.5.cloned.1.call-done, bf16[384,2048]{1,0:T(8,128)(2,1)S(1)} %copy-done.1, bf16[384,2048]{1,0:T(8,128)(2,1)S(1)} %copy-done), kind=kLoop, calls=%fused_computation.13 | loop fusion | flops 6291456 | bytes 6291456 | tf_op jit(solution)/shard_map/convert_element_type | solution.py:78
  (20 shorter events, 0.1 us)
Async XLA Ops:
  6.5 1.5 copy-start
  6.5 1.9 copy-start.3
  6.5 2.0 copy-start.2
  6.5 81.7 %all-gather.3.cloned.1.call-start = ((), (), s32[]{:S(2)}) async-start(), calls=%async_computation | async-start | bytes 5242880 | tf_op jit(solution)/shard_map/all_gather | solution.py:66
  7.3 161.8 %all-gather.5.cloned.1.call-start = ((), (), s32[]{:S(2)}) async-start(), calls=%async_computation.1 | async-start | bytes 5242880 | tf_op jit(solution)/shard_map/all_gather | solution.py:67
  8.0 209.4 %all-reduce.3.cloned.1.call-start = ((), (), s32[]{:S(2)}) async-start(), calls=%async_computation.2 | async-start | bytes 3145728 | tf_op jit(solution)/shard_map/psum | solution.py:77
  90.8 6.1 %collective-permute-start = (bf16[8,512]{1,0:T(8,128)(2,1)S(1)}, bf16[8,512]{1,0:T(8,128)(2,1)S(1)}, u32[]{:S(2)}, u32[]{:S(2)}) collective-permute-start(bf16[8,512]{1,0:T(8,128)(2,1)S(1)} %get-tuple-element.7), channel_id=1, source_target_pairs={{0,4},{4,8},{8,12},{1,5},{5,9},{9,13},{2,6},{6,10},{10,14},{3,7},{... | collective-permute-start | bytes 24584 | tf_op jit(solution)/shard_map/ppermute | solution.py:20
  94.9 4.4 %collective-permute-start.1 = (bf16[8,512]{1,0:T(8,128)(2,1)S(1)}, bf16[8,512]{1,0:T(8,128)(2,1)S(1)}, u32[]{:S(2)}, u32[]{:S(2)}) collective-permute-start(bf16[8,512]{1,0:T(8,128)(2,1)S(1)} %get-tuple-element.8), channel_id=1, source_target_pairs={{4,0},{8,4},{12,8},{5,1},{9,5},{13,9},{6,2},{10,6},{14,10},{7,3},{... | collective-permute-start | bytes 24584 | tf_op jit(solution)/shard_map/ppermute | solution.py:21
  174.3 111.3 %all-reduce.5.cloned.1.call-start = ((), (), s32[]{:S(2)}) async-start(), calls=%async_computation.3 | async-start | bytes 3145728 | tf_op jit(solution)/shard_map/psum | solution.py:77
  217.5 2.1 copy-start.1
  222.2 5.3 %collective-permute-start.2 = (bf16[8,512]{1,0:T(8,128)(2,1)S(1)}, bf16[8,512]{1,0:T(8,128)(2,1)S(1)}, u32[]{:S(2)}, u32[]{:S(2)}) collective-permute-start(bf16[8,512]{1,0:T(8,128)(2,1)S(1)} %get-tuple-element.5), channel_id=1, source_target_pairs={{0,4},{4,8},{8,12},{1,5},{5,9},{9,13},{2,6},{6,10},{10,14},{3,7},{... | collective-permute-start | bytes 24584 | tf_op jit(solution)/shard_map/ppermute | solution.py:20
  225.3 4.4 %collective-permute-start.3 = (bf16[8,512]{1,0:T(8,128)(2,1)S(1)}, bf16[8,512]{1,0:T(8,128)(2,1)S(1)}, u32[]{:S(2)}, u32[]{:S(2)}) collective-permute-start(bf16[8,512]{1,0:T(8,128)(2,1)S(1)} %get-tuple-element.6), channel_id=1, source_target_pairs={{4,0},{8,4},{12,8},{5,1},{9,5},{13,9},{6,2},{10,6},{14,10},{7,3},{... | collective-permute-start | bytes 24584 | tf_op jit(solution)/shard_map/ppermute | solution.py:21
Sparse Core Ops, SparseCore 0:
  8.9 79.2 all-gather.2
  89.8 79.2 all-gather.4
  174.4 42.9 all-reduce.2
  242.2 43.4 all-reduce.4
where the time goes:
time: 298 us; the launch traced here: 295 us
  waiting for transfers between devices  242 us (81%)
  matrix products  21.7 us (7%)
  between operations  13.4 us (4%)
  starting transfers between devices  11.4 us (4%)
  other arithmetic  6.97 us (2%)
    psum x2, waiting for transfers between devices, per_device(): summed = lax.psum(update.astype(jnp.bfloat16), 'tp').astype(jnp.float32)  86.7 us
    all_gather x1, waiting for transfers between devices, per_device(): lax.all_gather(entry_weight, 'sp', axis=1, tiled=True)  79.7 us
    all_gather x1, waiting for transfers between devices, per_device(): lax.all_gather(back_weight, 'sp', axis=2, tiled=True)  69.6 us
    dot_general x2, matrix products, per_device(): update = jnp.dot(mixed, back_local, preferred_element_type=jnp.float32)  16.5 us
    ppermute x2, starting transfers between devices, extended_2(): before = lax.ppermute(last, axis, up)  7.18 us
  transfers between devices with their start and end apart: 8, of which 6 were waited for; matrix products, arithmetic and copies ran while one was open for 1% of the time, Pallas kernels for 0%

commit v1 on v0

--- a/solution.py
+++ b/solution.py
@@ -1,13 +1,325 @@
+import functools
+
 import jax
 import jax.numpy as jnp
 from jax import lax
+from jax.experimental import pallas as pl
+from jax.experimental.pallas import tpu as pltpu
 from jax.sharding import PartitionSpec as P
 
+EPSILON = 1e-05
+MESH = pl.DeviceIdType.MESH
+LANES = 128
 GROUPS = 4
 LAYERS = 2
-
-
-EPSILON = 1e-05
+HALO = 16
+SUBS = 2
+
+
+def kernel(
+    sizes,
+    tok_ref, gain_ref, entry_ref, mix_ref, pgain_ref, back_ref,
+    out_ref,
+    went, wback, state, normed, ext, mixed, t_own, t_out, t_in, s_own, s_in,
+    zsend, zrecv, ysend, yrecv, hsend, hrecv, asend, arecv, bsend, brecv, csend, crecv, lsem,
+):
+    n_g, n_s, n_t = sizes
+    layers, depth, width = entry_ref.shape
+    rows, channels = tok_ref.shape
+    cols = back_ref.shape[2]
+    half = rows // 2
+    pairs = 2 if n_g % 2 == 0 else 1
+    g, s, t = lax.axis_index("grp"), lax.axis_index("sp"), lax.axis_index("tp")
+    h = lax.rem(g, pairs)
+    y_dev = {"grp": g + 1 - 2 * h}
+    core = lax.rem(t, 2)
+    chip = lax.rem(t // 2, 2)
+    core_dev = {"tp": t + 1 - 2 * core}
+    x_dev = {"tp": t + 2 - 4 * chip}
+    right, left = {"sp": s + 1}, {"sp": s - 1}
+    has_right, has_left = s < n_s - 1, s > 0
+
+    barrier = pltpu.get_barrier_semaphore()
+
+    def greet(device):
+        pl.semaphore_signal(barrier, inc=1, device_id=device, device_id_type=MESH)
+
+    greet(core_dev)
+    greet(x_dev)
+    if pairs == 2:
+        greet(y_dev)
+    pl.when(has_right)(lambda: greet(right))
+    pl.when(has_left)(lambda: greet(left))
+    pl.semaphore_wait(
+        barrier, 1 + pairs + has_right.astype(jnp.int32) + has_left.astype(jnp.int32)
+    )
+
+    block_rows = (depth, back_ref.shape[1])
+
+    def piece(m, o, part, c):
+        layer, which = divmod(m, 2)
+        size = block_rows[which] // (pairs * SUBS)
+        start = pl.multiple_of((part * SUBS + c) * size, size)
+        if which == 0:
+            return went.at[layer, pl.ds(pl.multiple_of(o * depth + start, size), size)]
+        return wback.at[layer, o, pl.ds(start, size)]
+
+    def own_piece(m, c):
+        layer, which = divmod(m, 2)
+        size = block_rows[which] // (pairs * SUBS)
+        ref = (entry_ref, back_ref)[which]
+        return ref.at[layer, pl.ds(pl.multiple_of((h * SUBS + c) * size, size), size)]
+
+    def z_copy(m, o, c, to_right, own=False):
+        return pltpu.make_async_remote_copy(
+            src_ref=own_piece(m, c) if own else piece(m, o, h, c),
+            dst_ref=piece(m, o, h, c),
+            send_sem=zsend.at[m, o, c, 0 if to_right else 1],
+            recv_sem=zrecv.at[m, o, c],
+            device_id=right if to_right else left,
+            device_id_type=MESH,
+        )
+
+    def y_copy(m, o, c, part):
+        return pltpu.make_async_remote_copy(
+            src_ref=piece(m, o, part, c),
+            dst_ref=piece(m, o, part, c),
+            send_sem=ysend.at[m, o, c],
+            recv_sem=yrecv.at[m, o, c],
+            device_id=y_dev,
+            device_id_type=MESH,
+        )
+
+    def send_own(m):
+        for c in range(SUBS):
+            pl.when(has_right)(lambda: z_copy(m, s, c, True, own=True).start())
+            pl.when(has_left)(lambda: z_copy(m, s, c, False, own=True).start())
+
+    def sides(d):
+        return ((s >= d, s - d, True, has_right), (s + d < n_s, s + d, False, has_left))
+
+    def forward(m, d):
+        for c in range(SUBS):
+            for there, o, to_right, onward in sides(d):
+                @pl.when(there)
+                def _():
+                    z_copy(m, o, c, to_right).wait_recv()
+                    pl.when(onward)(lambda: z_copy(m, o, c, to_right).start())
+                    if pairs == 2:
+                        y_copy(m, o, c, h).start()
+
+    def await_y(m, o):
+        if pairs == 2:
+            for c in range(SUBS):
+                y_copy(m, o, c, 1 - h).wait_recv()
+
+    def await_y_all(m):
+        for d in range(1, n_s):
+            for there, o, _, _ in sides(d):
+                pl.when(there)(lambda: await_y(m, o))
+
+    send_own(0)
+
+    locals_ = []
+    for layer in range(layers):
+        locals_.append(
+            pltpu.make_async_copy(
+                entry_ref.at[layer],
+                went.at[layer, pl.ds(pl.multiple_of(s * depth, depth), depth)],
+                lsem.at[2 * layer],
+            )
+        )
+        locals_.append(
+            pltpu.make_async_copy(back_ref.at[layer], wback.at[layer, s], lsem.at[2 * layer + 1])
+        )
+    for copy in locals_:
+        copy.start()
+    for o in range(n_s):
+        state[o] = tok_ref[:, o * cols:(o + 1) * cols]
+
+    def normalize(layer):
+        def body(i, carry):
+            at = pl.ds(pl.multiple_of(i * 32, 32), 32)
+            total = jnp.zeros((32, 1), jnp.float32)
+            for o in range(n_s):
+                value = state[o, at, :].astype(jnp.float32)
+                total = total + jnp.sum(value * value, axis=-1, keepdims=True)
+            scale = lax.rsqrt(total / channels + EPSILON)
+            for o in range(n_s):
+                value = state[o, at, :].astype(jnp.float32)
+                gain = gain_ref[layer:layer + 1, o * cols:(o + 1) * cols]
+                normed[at, o * cols:(o + 1) * cols] = (value * scale * gain).astype(jnp.bfloat16)
+            return carry
+
+        lax.fori_loop(0, rows // 32, body, 0)
+
+    def halo_copy(layer, to_right):
+        src = rows - HALO if to_right else 0
+        dst = rows if to_right else rows + HALO
+        side = 0 if to_right else 1
+        return pltpu.make_async_remote_copy(
+            src_ref=ext.at[layer, pl.ds(src, HALO)],
+            dst_ref=ext.at[layer, pl.ds(dst, HALO)],
+            send_sem=hsend.at[layer, side],
+            recv_sem=hrecv.at[layer, side],
+            device_id=right if to_right else left,
+            device_id_type=MESH,
+        )
+
+    def entry(layer):
+        ext[layer, 0:rows] = jnp.dot(
+            normed[...], went[layer], preferred_element_type=jnp.float32
+        ).astype(jnp.bfloat16)
+        pl.when(has_right)(lambda: halo_copy(layer, True).start())
+        pl.when(has_left)(lambda: halo_copy(layer, False).start())
+        zero = jnp.zeros((HALO, width), jnp.bfloat16)
+
+        @pl.when(s == 0)
+        def _():
+            ext[layer, rows:rows + HALO] = zero
+
+        @pl.when(s == n_s - 1)
+        def _():
+            ext[layer, rows + HALO:rows + 2 * HALO] = zero
+
+    def pool(layer):
+        pl.when(has_left)(lambda: halo_copy(layer, True).wait_recv())
+        pl.when(has_right)(lambda: halo_copy(layer, False).wait_recv())
+        reach = jnp.left_shift(jnp.int32(1), t)
+        shape = (rows, rows + 2 * HALO)
+        row = lax.broadcasted_iota(jnp.int32, shape, 0)
+        j = lax.broadcasted_iota(jnp.int32, shape, 1)
+        position = jnp.where(j < rows, j, jnp.where(j < rows + HALO, j - rows - HALO, j - HALO))
+        offset = position - row
+        band = jnp.where((offset >= -reach) & (offset < reach), 1.0, 0.0).astype(jnp.bfloat16)
+        summed = jnp.dot(band, ext[layer], preferred_element_type=jnp.float32)
+        at = s * rows + lax.broadcasted_iota(jnp.int32, (rows, 1), 0)
+        counted = jnp.minimum(at + reach, n_s * rows) - jnp.maximum(at - reach, 0)
+        means = summed / counted.astype(jnp.float32)
+        differ = (means - ext[layer, 0:rows].astype(jnp.float32)).astype(jnp.bfloat16)
+        product = jnp.dot(differ, mix_ref[layer, 0], preferred_element_type=jnp.float32)
+        mixed[...] = (product * pgain_ref[layer:layer + 1, :]).astype(jnp.bfloat16)
+
+    keep = pl.ds(pl.multiple_of(core * half, half), half)
+    give = pl.ds(pl.multiple_of((1 - core) * half, half), half)
+    turn = 1 - 2 * (s // ((n_s + 1) // 2))
+
+    def block_of(k):
+        return lax.rem(s + turn * k + n_s, n_s)
+
+    def a_copy(layer, k):
+        return pltpu.make_async_remote_copy(
+            src_ref=t_out.at[layer, k], dst_ref=t_in.at[layer, k],
+            send_sem=asend.at[layer, k], recv_sem=arecv.at[layer, k],
+            device_id=core_dev, device_id_type=MESH,
+        )
+
+    def b_copy(layer, k):
+        return pltpu.make_async_remote_copy(
+            src_ref=s_own.at[layer, k], dst_ref=s_in.at[layer, k],
+            send_sem=bsend.at[layer, k], recv_sem=brecv.at[layer, k],
+            device_id=x_dev, device_id_type=MESH,
+        )
+
+    def c_copy(layer, k, rows_at):
+        o = block_of(k)
+        return pltpu.make_async_remote_copy(
+            src_ref=state.at[o, rows_at], dst_ref=state.at[o, rows_at],
+            send_sem=csend.at[layer, k], recv_sem=crecv.at[layer, k],
+            device_id=core_dev, device_id_type=MESH,
+        )
+
+    def back(layer, k):
+        o = block_of(k)
+        if k > 0:
+            await_y(2 * layer + 1, o)
+        weight = wback[layer, o]
+        t_out[layer, k] = jnp.dot(
+            mixed[give, :], weight, preferred_element_type=jnp.float32
+        ).astype(jnp.bfloat16)
+        a_copy(layer, k).start()
+        t_own[...] = jnp.dot(mixed[keep, :], weight, preferred_element_type=jnp.float32).astype(
+            jnp.bfloat16
+        )
+        a_copy(layer, k).wait_recv()
+        s_own[layer, k] = (
+            t_own[...].astype(jnp.float32) + t_in[layer, k].astype(jnp.float32)
+        ).astype(jnp.bfloat16)
+        b_copy(layer, k).start()
+
+    def finish(layer, k):
+        o = block_of(k)
+        b_copy(layer, k).wait_recv()
+        state[o, keep] = (
+            state[o, keep].astype(jnp.float32)
+            + (s_own[layer, k].astype(jnp.float32) + s_in[layer, k].astype(jnp.float32))
+        ).astype(jnp.bfloat16)
+        c_copy(layer, k, keep).start()
+
+    def settle(layer):
+        for k in range(n_s):
+            c_copy(layer, k, give).wait_recv()
+            c_copy(layer, k, keep).wait_send()
+
+    normalize(0)
+    for d in range(1, n_s):
+        forward(0, d)
+    for layer in range(layers):
+        m = 2 * layer
+        send_own(m + 1)
+        if layer == 0:
+            for copy in locals_:
+                copy.wait()
+        forward(m + 1, 1)
+        await_y_all(m)
+        entry(layer)
+        for d in range(2, n_s - 1):
+            forward(m + 1, d)
+        pool(layer)
+        last = layer == layers - 1
+        if last:
+            back(layer, 0)
+            back(layer, 1)
+        for d in range(max(2, n_s - 1), n_s):
+            forward(m + 1, d)
+        if not last:
+            send_own(m + 2)
+            back(layer, 0)
+            back(layer, 1)
+            forward(m + 2, 1)
+        for k in range(2, n_s):
+            back(layer, k)
+        if not last and n_s > 2:
+            forward(m + 2, 2)
+        for k in range(n_s):
+            finish(layer, k)
+        if not last:
+            for d in range(3, n_s):
+                forward(m + 2, d)
+        settle(layer)
+        if not last:
+            normalize(layer + 1)
+
+    for o in range(n_s):
+        out_ref[:, o * cols:(o + 1) * cols] = state[o]
+
+    for layer in range(layers):
+        pl.when(has_right)(lambda: halo_copy(layer, True).wait_send())
+        pl.when(has_left)(lambda: halo_copy(layer, False).wait_send())
+        for k in range(n_s):
+            a_copy(layer, k).wait_send()
+            b_copy(layer, k).wait_send()
+    for m in range(2 * layers):
+        for c in range(SUBS):
+            pl.when(has_right)(lambda: z_copy(m, s, c, True, own=True).wait_send())
+            pl.when(has_left)(lambda: z_copy(m, s, c, False, own=True).wait_send())
+            for d in range(1, n_s):
+                for there, o, to_right, onward in sides(d):
+                    @pl.when(there)
+                    def _():
+                        pl.when(onward)(lambda: z_copy(m, o, c, to_right).wait_send())
+                        if pairs == 2:
+                            y_copy(m, o, c, h).wait_send()
 
 
 def extended_2(value, sides, width):
@@ -59,7 +371,7 @@
     return (mixed.reshape(row_count, group_here * width) * gain_layer).astype(jnp.bfloat16)
 
 
-def per_device(tokens, norm_gain, entry_weight, mix_weight, pool_gain, back_weight):
+def plain(tokens, norm_gain, entry_weight, mix_weight, pool_gain, back_weight):
     reach = 2 ** (GROUPS - 1)
     state = tokens
     entry_all, back_all = (
@@ -80,6 +392,52 @@
 
 
 def solution(mesh):
+    n_g, n_s, n_t = mesh.shape["grp"], mesh.shape["sp"], mesh.shape["tp"]
+
+    def per_device(tokens, norm_gain, entry_weight, mix_weight, pool_gain, back_weight):
+        layers, depth, width = entry_weight.shape
+        rows, channels = tokens.shape
+        cols = back_weight.shape[2]
+        half = rows // 2
+        if n_t != 4 or cols % LANES or depth % LANES or rows % (2 * HALO):
+            return plain(tokens, norm_gain, entry_weight, mix_weight, pool_gain, back_weight)
+        bf16 = jnp.bfloat16
+        dma = pltpu.SemaphoreType.DMA
+        flow = pltpu.VMEM((layers, n_s, half, cols), bf16)
+        vmem = pl.BlockSpec(memory_space=pltpu.VMEM)
+        return pl.pallas_call(
+            functools.partial(kernel, (n_g, n_s, n_t)),
+            out_shape=jax.ShapeDtypeStruct((rows, channels), bf16),
+            in_specs=[vmem] * 6,
+            out_specs=vmem,
+            scratch_shapes=[
+                pltpu.VMEM((layers, n_s * depth, width), bf16),
+                pltpu.VMEM((layers, n_s, back_weight.shape[1], cols), bf16),
+                pltpu.VMEM((n_s, rows, cols), bf16),
+                pltpu.VMEM((rows, channels), bf16),
+                pltpu.VMEM((layers, rows + 2 * HALO, width), bf16),
+                pltpu.VMEM((rows, width), bf16),
+                pltpu.VMEM((half, cols), bf16),
+                flow, flow, flow, flow,
+                dma((2 * layers, n_s, SUBS, 2)),
+                dma((2 * layers, n_s, SUBS)),
+                dma((2 * layers, n_s, SUBS)),
+                dma((2 * layers, n_s, SUBS)),
+                dma((layers, 2)),
+                dma((layers, 2)),
+                dma((layers, n_s)),
+                dma((layers, n_s)),
+                dma((layers, n_s)),
+                dma((layers, n_s)),
+                dma((layers, n_s)),
+                dma((layers, n_s)),
+                dma((2 * layers,)),
+            ],
+            compiler_params=pltpu.CompilerParams(
+                collective_id=0, has_side_effects=True, vmem_limit_bytes=56 * 1024 * 1024
+            ),
+        )(tokens, norm_gain, entry_weight, mix_weight, pool_gain, back_weight)
+
     return jax.shard_map(
         per_device,
         mesh=mesh,

time: 298 us -> 107 us (0.36)
  waiting for transfers between devices: 242 us -> 0 us
  Pallas kernels: 0 us -> 104 us
  matrix products: 21.7 us -> 0 us
  between operations: 13.4 us -> 0.01 us
  starting transfers between devices: 11.4 us -> 0 us
  other arithmetic: 6.97 us -> 0 us
    all_gather x2 -> x0, waiting for transfers between devices: 149 us -> none  [the longest x1 79.7 us: per_device(): lax.all_gather(entry_weight, 'sp', axis=1, tiled=True)]
    pallas_call x0 -> x1, Pallas kernels: none -> 104 us  [per_device(): pl.pallas_call(functools.partial(kernel, (n_g, n_s, n_t)), out_shape=jax....]
    psum x2 -> x0, waiting for transfers between devices: 86.7 us -> none  [per_device(): summed = lax.psum(update.astype(jnp.bfloat16), 'tp').astype(jnp.float32)]
    dot_general x4 -> x0, matrix products: 21.7 us -> none  [the longest x2 16.5 us: per_device(): update = jnp.dot(mixed, back_local, preferred_element_type=jnp.float32)]
    ppermute x4 -> x0, starting transfers between devices: 11.3 us -> none  [the longest x2 7.18 us: extended_2(): before = lax.ppermute(last, axis, up)]
    ppermute x4 -> x0, waiting for transfers between devices: 4.54 us -> none  [the longest x2 4.53 us: extended_2(): after = lax.ppermute(first, axis, down)]
    convert_element_type x4 -> x0, other arithmetic: 4.46 us -> none  [the longest x1 3.35 us: per_device(): state = (state.astype(jnp.float32) + summed).astype(jnp.bfloat16)]
  transfers between devices with their start and end apart: 8 -> 0, of which waited for: 6 -> 0; matrix products, arithmetic and copies ran while one was open for 1% -> 0% of each run, Pallas kernels for 0% -> 0%
where the time goes in v1:
time: 107 us
  Pallas kernels  104 us (97%)
  local copies, waits for them, and re-layouts  2.73 us (3%)
    pallas_call x1, Pallas kernels, per_device(): pl.pallas_call(functools.partial(kernel, (n_g, n_s, n_t)), out_shape=jax....  104 us
    unnamed x1, local copies, waits for them, and re-layouts  2.73 us

profile of v1, /device:TPU:11, one launch (start us, length us, event | category | flops | bytes accessed | tf_op | source)
XLA Modules:
  0.0 107.0 jit_solution(4757891709861326625)
XLA Ops:
  0.0 104.2 %shard_map.64 = bf16[384,2048]{1,0:T(8,128)(2,1)} custom-call(bf16[384,2048]{1,0:T(8,128)(2,1)} %tok_ref.1, f32[2,2048]{1,0:T(2,128)} %gain_ref.1, bf16[2,512,512]{2,1,0:T(8,128)(2,1)} %entry_ref.1, bf16[2,1,512,512]{3,2,1,0:T(8,128)(2,1)} %mix_ref.1, f32[2,512]{1,0:T(2,128)} %pgain_ref.1, bf16[2,512,512]{2,1,0:T(8,128)(2,1)} %back_ref.1), custom_call_target="tpu_custom_call" | custom-call | tf_op jit(solution)/shard_map/pallas_call | solution.py:408
  104.2 2.7 %copy.8 = bf16[384,2048]{1,0:T(8,128)(2,1)} copy(bf16[384,2048]{1,0:T(8,128)(2,1)} %shard_map.64) | data formatting | bytes 3145728

commit v2 on v1

--- a/solution.py
+++ b/solution.py
@@ -18,10 +18,10 @@
 
 def kernel(
     sizes,
-    tok_ref, gain_ref, entry_ref, mix_ref, pgain_ref, back_ref,
+    tok_ref, gain_ref, entry_ref, mix_hbm, pgain_ref, back_ref,
     out_ref,
-    went, wback, state, normed, ext, mixed, t_own, t_out, t_in, s_own, s_in,
-    zsend, zrecv, ysend, yrecv, hsend, hrecv, asend, arecv, bsend, brecv, csend, crecv, lsem,
+    mix_ref, went, wback, state, normed, ext, mixed, t_own, t_out, t_in, s_own, s_in,
+    zsend, zrecv, ysend, yrecv, hsend, hrecv, asend, arecv, bsend, brecv, csend, crecv, lsem, osem,
 ):
     n_g, n_s, n_t = sizes
     layers, depth, width = entry_ref.shape
@@ -120,22 +120,20 @@
 
     send_own(0)
 
-    locals_ = []
+    locals_ = [pltpu.make_async_copy(mix_hbm, mix_ref, lsem.at[0])]
     for layer in range(layers):
-        locals_.append(
-            pltpu.make_async_copy(
-                entry_ref.at[layer],
-                went.at[layer, pl.ds(pl.multiple_of(s * depth, depth), depth)],
-                lsem.at[2 * layer],
-            )
-        )
-        locals_.append(
-            pltpu.make_async_copy(back_ref.at[layer], wback.at[layer, s], lsem.at[2 * layer + 1])
-        )
-    for copy in locals_:
+        own = went.at[layer, pl.ds(pl.multiple_of(s * depth, depth), depth)]
+        locals_.append(pltpu.make_async_copy(entry_ref.at[layer], own, lsem.at[2 * layer + 1]))
+        own = wback.at[layer, s]
+        locals_.append(pltpu.make_async_copy(back_ref.at[layer], own, lsem.at[2 * layer + 2]))
+    tokens_in = [
+        pltpu.make_async_copy(
+            tok_ref.at[:, pl.ds(o * cols, cols)], state.at[o], lsem.at[2 * layers + 1 + o]
+        )
+        for o in range(n_s)
+    ]
+    for copy in tokens_in + locals_:
         copy.start()
-    for o in range(n_s):
-        state[o] = tok_ref[:, o * cols:(o + 1) * cols]
 
     def normalize(layer):
         def body(i, carry):
@@ -238,12 +236,14 @@
             mixed[give, :], weight, preferred_element_type=jnp.float32
         ).astype(jnp.bfloat16)
         a_copy(layer, k).start()
-        t_own[...] = jnp.dot(mixed[keep, :], weight, preferred_element_type=jnp.float32).astype(
-            jnp.bfloat16
-        )
+        t_own[layer, k] = jnp.dot(
+            mixed[keep, :], weight, preferred_element_type=jnp.float32
+        ).astype(jnp.bfloat16)
+
+    def join(layer, k):
         a_copy(layer, k).wait_recv()
         s_own[layer, k] = (
-            t_own[...].astype(jnp.float32) + t_in[layer, k].astype(jnp.float32)
+            t_own[layer, k].astype(jnp.float32) + t_in[layer, k].astype(jnp.float32)
         ).astype(jnp.bfloat16)
         b_copy(layer, k).start()
 
@@ -256,52 +256,65 @@
         ).astype(jnp.bfloat16)
         c_copy(layer, k, keep).start()
 
+    def out_copy(k):
+        o = block_of(k)
+        return pltpu.make_async_copy(
+            state.at[o],
+            out_ref.at[:, pl.ds(pl.multiple_of(o * cols, cols), cols)],
+            osem.at[k],
+        )
+
     def settle(layer):
         for k in range(n_s):
             c_copy(layer, k, give).wait_recv()
+            if layer == layers - 1:
+                out_copy(k).start()
             c_copy(layer, k, keep).wait_send()
 
+    early = max(1, n_s - 2)
+
+    def gather(m, first, last):
+        for d in range(first, last):
+            forward(m, d)
+            if d == early and m + 1 < 2 * layers:
+                send_own(m + 1)
+
+    for copy in tokens_in:
+        copy.wait()
     normalize(0)
-    for d in range(1, n_s):
-        forward(0, d)
+    gather(0, 1, n_s)
     for layer in range(layers):
         m = 2 * layer
-        send_own(m + 1)
+        last = layer == layers - 1
+        gather(m + 1, 1, 2)
         if layer == 0:
             for copy in locals_:
                 copy.wait()
-        forward(m + 1, 1)
         await_y_all(m)
         entry(layer)
-        for d in range(2, n_s - 1):
-            forward(m + 1, d)
+        gather(m + 1, 2, early + 1)
         pool(layer)
-        last = layer == layers - 1
-        if last:
-            back(layer, 0)
-            back(layer, 1)
-        for d in range(max(2, n_s - 1), n_s):
-            forward(m + 1, d)
+        for k in range(n_s):
+            if k == min(2, n_s - 1):
+                gather(m + 1, early + 1, n_s)
+                if not last:
+                    gather(m + 2, 1, 2)
+            back(layer, k)
+            if k > 0:
+                join(layer, k - 1)
+        join(layer, n_s - 1)
         if not last:
-            send_own(m + 2)
-            back(layer, 0)
-            back(layer, 1)
-            forward(m + 2, 1)
-        for k in range(2, n_s):
-            back(layer, k)
-        if not last and n_s > 2:
-            forward(m + 2, 2)
+            gather(m + 2, 2, early + 1)
         for k in range(n_s):
             finish(layer, k)
         if not last:
-            for d in range(3, n_s):
-                forward(m + 2, d)
+            gather(m + 2, early + 1, n_s)
         settle(layer)
         if not last:
             normalize(layer + 1)
 
-    for o in range(n_s):
-        out_ref[:, o * cols:(o + 1) * cols] = state[o]
+    for k in range(n_s):
+        out_copy(k).wait()
 
     for layer in range(layers):
         pl.when(has_right)(lambda: halo_copy(layer, True).wait_send())
@@ -405,20 +418,21 @@
         dma = pltpu.SemaphoreType.DMA
         flow = pltpu.VMEM((layers, n_s, half, cols), bf16)
         vmem = pl.BlockSpec(memory_space=pltpu.VMEM)
+        hbm = pl.BlockSpec(memory_space=pl.ANY)
         return pl.pallas_call(
             functools.partial(kernel, (n_g, n_s, n_t)),
             out_shape=jax.ShapeDtypeStruct((rows, channels), bf16),
-            in_specs=[vmem] * 6,
-            out_specs=vmem,
+            in_specs=[hbm, vmem, hbm, hbm, vmem, hbm],
+            out_specs=hbm,
             scratch_shapes=[
+                pltpu.VMEM(mix_weight.shape, bf16),
                 pltpu.VMEM((layers, n_s * depth, width), bf16),
                 pltpu.VMEM((layers, n_s, back_weight.shape[1], cols), bf16),
                 pltpu.VMEM((n_s, rows, cols), bf16),
                 pltpu.VMEM((rows, channels), bf16),
                 pltpu.VMEM((layers, rows + 2 * HALO, width), bf16),
                 pltpu.VMEM((rows, width), bf16),
-                pltpu.VMEM((half, cols), bf16),
-                flow, flow, flow, flow,
+                flow, flow, flow, flow, flow,
                 dma((2 * layers, n_s, SUBS, 2)),
                 dma((2 * layers, n_s, SUBS)),
                 dma((2 * layers, n_s, SUBS)),
@@ -431,7 +445,8 @@
                 dma((layers, n_s)),
                 dma((layers, n_s)),
                 dma((layers, n_s)),
-                dma((2 * layers,)),
+                dma((2 * layers + 1 + n_s,)),
+                dma((n_s,)),
             ],
             compiler_params=pltpu.CompilerParams(
                 collective_id=0, has_side_effects=True, vmem_limit_bytes=56 * 1024 * 1024

time: 107 us -> 102 us (0.953)
  Pallas kernels: 104 us -> 98.5 us
    pallas_call x1, Pallas kernels: 104 us -> 98.5 us  [per_device(): pl.pallas_call(functools.partial(kernel, (n_g, n_s, n_t)), out_shape=jax....]
where the time goes in v2:
time: 102 us; the launch traced here: 101 us
  Pallas kernels  98.5 us (97%)
  local copies, waits for them, and re-layouts  2.73 us (3%)
    pallas_call x1, Pallas kernels, per_device(): pl.pallas_call(functools.partial(kernel, (n_g, n_s, n_t)), out_shape=jax....  98.5 us
    unnamed x1, local copies, waits for them, and re-layouts  2.73 us

profile of v2, /device:TPU:11, one launch (start us, length us, event | category | flops | bytes accessed | tf_op | source)
XLA Modules:
  0.0 101.3 jit_solution(6528668720763063250)
XLA Ops:
  0.0 98.5 %shard_map.64 = bf16[384,2048]{1,0:T(8,128)(2,1)} custom-call(bf16[384,2048]{1,0:T(8,128)(2,1)} %tok_ref.1, f32[2,2048]{1,0:T(2,128)} %gain_ref.1, bf16[2,512,512]{2,1,0:T(8,128)(2,1)} %entry_ref.1, bf16[2,1,512,512]{3,2,1,0:T(8,128)(2,1)} %mix_hbm.1, f32[2,512]{1,0:T(2,128)} %pgain_ref.1, bf16[2,512,512]{2,1,0:T(8,128)(2,1)} %back_ref.1), custom_call_target="tpu_custom_call" | custom-call | tf_op jit(solution)/shard_map/pallas_call | solution.py:422
  98.5 2.7 %copy.8 = bf16[384,2048]{1,0:T(8,128)(2,1)} copy(bf16[384,2048]{1,0:T(8,128)(2,1)} %shard_map.64) | data formatting | bytes 3145728

commit v3 on v2

--- a/solution.py
+++ b/solution.py
@@ -304,11 +304,9 @@
                 join(layer, k - 1)
         join(layer, n_s - 1)
         if not last:
-            gather(m + 2, 2, early + 1)
+            gather(m + 2, 2, n_s)
         for k in range(n_s):
             finish(layer, k)
-        if not last:
-            gather(m + 2, early + 1, n_s)
         settle(layer)
         if not last:
             normalize(layer + 1)

time: 102 us -> 102 us (level)
  no operation moved by 1% of the time
where the time goes in v3:
time: 102 us; the launch traced here: 101 us
  Pallas kernels  98.5 us (97%)
  local copies, waits for them, and re-layouts  2.73 us (3%)
    pallas_call x1, Pallas kernels, per_device(): pl.pallas_call(functools.partial(kernel, (n_g, n_s, n_t)), out_shape=jax....  98.5 us
    unnamed x1, local copies, waits for them, and re-layouts  2.73 us

profile of v3, /device:TPU:11, one launch (start us, length us, event | category | flops | bytes accessed | tf_op | source)
XLA Modules:
  0.0 101.3 jit_solution(14086237548803720161)
XLA Ops:
  0.0 98.5 %shard_map.64 = bf16[384,2048]{1,0:T(8,128)(2,1)} custom-call(bf16[384,2048]{1,0:T(8,128)(2,1)} %tok_ref.1, f32[2,2048]{1,0:T(2,128)} %gain_ref.1, bf16[2,512,512]{2,1,0:T(8,128)(2,1)} %entry_ref.1, bf16[2,1,512,512]{3,2,1,0:T(8,128)(2,1)} %mix_hbm.1, f32[2,512]{1,0:T(2,128)} %pgain_ref.1, bf16[2,512,512]{2,1,0:T(8,128)(2,1)} %back_ref.1), custom_call_target="tpu_custom_call" | custom-call | tf_op jit(solution)/shard_map/pallas_call | solution.py:420
  98.5 2.7 %copy.8 = bf16[384,2048]{1,0:T(8,128)(2,1)} copy(bf16[384,2048]{1,0:T(8,128)(2,1)} %shard_map.64) | data formatting | bytes 3145728
